TPU v7x, 512 devices: a 8x2x16 block of a 8x8x16 slice. The times are simulated.
512 devices in a mesh: grp: 2 (over y), sp: 32 (over z, core), tp: 8 (over x).
Axes of the slice: x: 8, y: 2, z: 16, core: 2. Of those that a mesh axis runs over, the one named last changes fastest.
The devices are a block of a 8x8x16 slice.
Arguments:
- tokens: bfloat16 [32768, 2048], P(('grp', 'sp'), 'tp'), parts along dimension 0, may hold values from -140 to 140, as said below
- mix_gain: bfloat16 [2, 2048], replicated, may hold values from 0.099609375 to 1.8984375
- gate_weight: bfloat16 [2, 2048, 2048], P(None, 'sp', 'tp'), may hold values from -0.125 to 0.125
- mix_weight: bfloat16 [2, 2048, 2048], P(None, 'sp', 'tp'), may hold values from -0.125 to 0.125
- value_weight: bfloat16 [2, 2048, 2048], P(None, 'sp', 'tp'), may hold values from -0.125 to 0.125
- out_weight: bfloat16 [2, 2048, 2048], P(None, 'sp', 'tp'), may hold values from -0.125 to 0.125
- conv_taps: bfloat16 [2, 3, 2048], P(None, None, 'tp'), may hold values from -3.5 to 3.5
Outputs:
- result_stream: bfloat16 [32768, 2048], P(('grp', 'sp'), 'tp'), parts along dimension 0
There are 2 independent parts, one for each index of `grp`. A program takes and returns all parts, laid end to end along the dimension named above; an argument that names none is the same for every part. Nothing has to cross between parts.
Inputs may be any that keep to these rules, and one draw needn't show every extreme that they name: `tokens`: activations with feature scales of several sizes.
All inputs are finite; a program needn't handle non-finite values.
Results may differ from a plain program's by a relative error of at most 0.015.
Values may be sent and summed in bfloat16 or wider, within the bound.
No kernel may reach another device: no remote copies, remote signals or barrier semaphores. Data moves between devices by JAX's collectives and lax.ppermute only.
A program may use at most 64 MiB of HBM per device.

v0:
```python
import jax
import jax.numpy as jnp
from jax import lax
from jax.sharding import PartitionSpec as P

EPS = 1e-06


def passed_along(x, axis, by):
    devices = lax.axis_size(axis)
    pairs = [(i, i + by) for i in range(devices) if 0 <= i + by < devices]
    return lax.ppermute(x, axis, pairs)


def in_one_piece(arrays, axis, dim, along):
    ends, at = ([], 0)
    for a in arrays[:-1]:
        at += a.shape[along]
        ends.append(at)
    both = jnp.concatenate(arrays, axis=along)
    return tuple(jnp.split(lax.all_gather(both, axis, axis=dim, tiled=True), ends, axis=along))


def in_order(pieces, dim):
    dims = list(pieces.shape[1:])
    dims[dim] *= pieces.shape[0]
    return jnp.moveaxis(pieces, 0, dim).reshape(dims)


def copy_for_each(x, axis):
    copies = jnp.broadcast_to(x, (lax.axis_size(axis), *x.shape))
    return lax.all_to_all(copies, axis, split_axis=0, concat_axis=0, tiled=True)


def collect(x, axis, dim):
    return in_order(copy_for_each(x, axis), dim)


def normed_rows(rows, gain):
    wide_rows = rows.astype(jnp.float32)
    factor = lax.rsqrt(jnp.mean(wide_rows * wide_rows, axis=1, keepdims=True) + EPS)
    return (wide_rows * factor * gain.astype(jnp.float32)).astype(jnp.bfloat16)


def convolve(carried, before, tap_rows):
    padded = jnp.concatenate([before, carried], axis=0)
    row_count = carried.shape[0]
    result = jnp.zeros_like(carried)
    for tap_index in range(tap_rows.shape[0]):
        result = (
            result
            + tap_rows[tap_index].astype(jnp.float32) * padded[tap_index : tap_index + row_count]
        )
    return result


def shards(tokens, mix_gain, gate_weight, mix_weight, value_weight, out_weight, conv_taps):
    layer_count = gate_weight.shape[0]
    conv_reach = conv_taps.shape[1] - 1
    fringe_depth = conv_reach * layer_count
    before_rows = passed_along(tokens[tokens.shape[0] - fringe_depth :], "sp", 1)
    stream = jnp.concatenate([before_rows, tokens], axis=0)
    gathered = in_one_piece((gate_weight, mix_weight, value_weight, out_weight), "sp", 1, 0)
    channels = gate_weight.shape[2]
    for layer_index in range(layer_count):
        whole = collect(stream, "tp", 1)
        normed = normed_rows(whole, mix_gain[layer_index])
        gate = jnp.dot(normed, gathered[0][layer_index], preferred_element_type=jnp.float32)
        inner = jnp.dot(normed, gathered[1][layer_index], preferred_element_type=jnp.float32)
        values = jnp.dot(normed, gathered[2][layer_index], preferred_element_type=jnp.float32)
        gate = gate.astype(jnp.bfloat16)
        inner = inner.astype(jnp.bfloat16)
        values = values.astype(jnp.bfloat16)
        carried = inner.astype(jnp.float32) * values.astype(jnp.float32)
        before = jnp.zeros((conv_reach, channels), jnp.float32)
        conv = convolve(carried, before, conv_taps[layer_index])
        mixed = (gate.astype(jnp.float32) * conv).astype(jnp.bfloat16)
        mixed_all = lax.all_gather(mixed, "tp", axis=1, tiled=True)
        product = jnp.dot(mixed_all, gathered[3][layer_index], preferred_element_type=jnp.float32)
        stream = (stream.astype(jnp.float32) + product).astype(jnp.bfloat16)
    return stream[fringe_depth:]


def solution(mesh):
    return jax.shard_map(
        shards,
        mesh=mesh,
        in_specs=(
            P(("grp", "sp"), "tp"),
            P(),
            P(None, "sp", "tp"),
            P(None, "sp", "tp"),
            P(None, "sp", "tp"),
            P(None, "sp", "tp"),
            P(None, None, "tp"),
        ),
        out_specs=P(("grp", "sp"), "tp"),
        check_vma=False,
    )
```

profile of v0, /device:TPU:66, one launch (start us, length us, event | category | flops | bytes accessed | tf_op | source)
XLA Modules:
  0.0 306.0 jit_solution(15098368979078359198)
XLA Ops:
  6.6 1.7 pad_maximum_fusion.1
  8.3 0.7 slice.88
  9.0 1.8 collective-permute-start
  10.8 0.8 collective-permute-done
  11.6 1.0 pad_maximum_fusion
  12.6 1.5 broadcast_in_dim.4
  14.1 43.5 %all-to-all-start = ((bf16[8,516,256]{2,1,0:T(8,128)(2,1)}), bf16[8,516,256]{2,1,0:T(8,128)(2,1)S(1)}, u32[]{:S(2)}, u32[]{:S(2)}) async-start(bf16[8,516,256]{2,1,0:T(8,128)(2,1)} %broadcast_in_dim.4), calls=%async_computation | async-start | bytes 4259840 | tf_op jit(solution)/shard_map/all_to_all | solution.py:32
  57.8 51.2 %all-to-all-done = bf16[8,516,256]{2,1,0:T(8,128)(2,1)S(1)} async-done(((bf16[8,516,256]{2,1,0:T(8,128)(2,1)}), bf16[8,516,256]{2,1,0:T(8,128)(2,1)S(1)}, u32[]{:S(2)}, u32[]{:S(2)}) %all-to-all-start) | async-done | bytes 2113568 | tf_op jit(solution)/shard_map/all_to_all | solution.py:32
  109.0 0.5 fusion
  109.5 0.6 fusion.7
  110.0 0.4 copy.8
  110.5 0.1 pad.8
  110.6 0.7 copy.10
  111.3 12.6 %all-gather.4.cloned.1.call-done = bf16[8,2048,256]{2,1,0:T(8,128)(2,1)} async-done(((bf16[8,64,256]{2,1,0:T(8,128)(2,1)}), bf16[8,2048,256]{2,1,0:T(8,128)(2,1)}) %all-gather.4.cloned.1.call-update) | async-done | bytes 8388624 | tf_op jit(solution)/shard_map/all_gather | solution.py:21
  123.9 2.0 fusion.13
  125.9 2.0 fusion.12
  128.0 2.7 fusion.10
  130.8 49.9 %all-gather.6.cloned.1.call-done = bf16[516,2048]{1,0:T(8,128)(2,1)} async-done(((bf16[516,256]{1,0:T(8,128)(2,1)}), bf16[516,2048]{1,0:T(8,128)(2,1)}) %all-gather.6.cloned.1.call-update) | async-done | bytes 2113552 | tf_op jit(solution)/shard_map/all_gather | solution.py:78
  180.7 2.6 add_convert_fusion
  183.3 1.5 broadcast_in_dim.5
  184.8 5.6 %all-to-all-start.1 = ((bf16[8,516,256]{2,1,0:T(8,128)(2,1)}), bf16[8,516,256]{2,1,0:T(8,128)(2,1)S(1)}, u32[]{:S(2)}, u32[]{:S(2)}) async-start(bf16[8,516,256]{2,1,0:T(8,128)(2,1)} %broadcast_in_dim.5), calls=%async_computation.1 | async-start | bytes 4259840 | tf_op jit(solution)/shard_map/all_to_all | solution.py:32
  190.3 45.0 %all-to-all-done.1 = bf16[8,516,256]{2,1,0:T(8,128)(2,1)S(1)} async-done(((bf16[8,516,256]{2,1,0:T(8,128)(2,1)}), bf16[8,516,256]{2,1,0:T(8,128)(2,1)S(1)}, u32[]{:S(2)}, u32[]{:S(2)}) %all-to-all-start.1) | async-done | bytes 2113568 | tf_op jit(solution)/shard_map/all_to_all | solution.py:32
  235.3 0.5 fusion.3
  235.9 0.6 fusion.6
  236.4 0.4 copy.9
  237.0 0.7 copy.11
  237.7 2.0 fusion.19
  239.7 2.0 fusion.18
  241.7 2.7 fusion.16
  244.5 51.6 %all-gather.8.cloned.1.call-done = bf16[516,2048]{1,0:T(8,128)(2,1)} async-done(((bf16[516,256]{1,0:T(8,128)(2,1)}), bf16[516,2048]{1,0:T(8,128)(2,1)}) %all-gather.8.cloned.1.call-update) | async-done | bytes 2113552 | tf_op jit(solution)/shard_map/all_gather | solution.py:78
  296.0 2.6 fusion.20
  298.6 0.8 fusion.22
  (19 shorter events, 0.4 us)
Async XLA Ops:
  6.5 117.4 %all-gather.4.cloned.1.call-start = ((), (), s32[]{:S(2)}) async-start(), calls=%async_computation.2 | async-start | bytes 8650752 | tf_op jit(solution)/shard_map/all_gather | solution.py:21
  9.0 2.6 collective-permute-start
  14.1 43.5 %copy-start.1 = (bf16[2,2048]{1,0:T(2,128)(2,1)S(1)}, bf16[2,2048]{1,0:T(2,128)(2,1)}, u32[]{:S(2)}) copy-start(bf16[2,2048]{1,0:T(2,128)(2,1)} %param.8) | copy-start | bytes 24580
  14.1 43.6 %copy-start.2 = (bf16[2,3,256]{2,0,1:T(2,128)(2,1)S(1)}, bf16[2,3,256]{2,0,1:T(2,128)(2,1)}, u32[]{:S(2)}) copy-start(bf16[2,3,256]{2,0,1:T(2,128)(2,1)} %param.13) | copy-start | bytes 9220
  14.1 94.8 %all-to-all-start = ((bf16[8,516,256]{2,1,0:T(8,128)(2,1)}), bf16[8,516,256]{2,1,0:T(8,128)(2,1)S(1)}, u32[]{:S(2)}, u32[]{:S(2)}) async-start(bf16[8,516,256]{2,1,0:T(8,128)(2,1)} %broadcast_in_dim.4), calls=%async_computation | async-start | bytes 4259840 | tf_op jit(solution)/shard_map/all_to_all | solution.py:32
  57.7 123.0 %all-gather.6.cloned.1.call-start = ((), (), s32[]{:S(2)}) async-start(), calls=%async_computation.3 | async-start | bytes 2396160 | tf_op jit(solution)/shard_map/all_gather | solution.py:78
  127.9 52.7 %copy-start = (bf16[512,256]{1,0:T(8,128)(2,1)S(1)}, bf16[512,256]{1,0:T(8,128)(2,1)}, u32[]{:S(2)}) copy-start(bf16[512,256]{1,0:T(8,128)(2,1)} %param.7) | copy-start | bytes 786436
  184.8 50.6 %all-to-all-start.1 = ((bf16[8,516,256]{2,1,0:T(8,128)(2,1)}), bf16[8,516,256]{2,1,0:T(8,128)(2,1)S(1)}, u32[]{:S(2)}, u32[]{:S(2)}) async-start(bf16[8,516,256]{2,1,0:T(8,128)(2,1)} %broadcast_in_dim.5), calls=%async_computation.1 | async-start | bytes 4259840 | tf_op jit(solution)/shard_map/all_to_all | solution.py:32
  190.3 105.7 %all-gather.8.cloned.1.call-start = ((), (), s32[]{:S(2)}) async-start(), calls=%async_computation.4 | async-start | bytes 2396160 | tf_op jit(solution)/shard_map/all_gather | solution.py:78
Sparse Core Ops, SparseCore 0:
  9.5 114.3 all-gather.3
  130.9 49.7 all-gather.5
  244.6 51.3 all-gather.7
where the time goes:
time: 307 us; the launch traced here: 306 us
  waiting for transfers between devices  211 us (69%)
  starting transfers between devices  50.9 us (17%)
  matrix products  18.6 us (6%)
  between operations  13.3 us (4%)
  local copies, waits for them, and re-layouts  6.28 us (2%)
  other arithmetic  5.67 us (2%)
    all_gather x2, waiting for transfers between devices, shards(): mixed_all = lax.all_gather(mixed, 'tp', axis=1, tiled=True)  101 us
    all_to_all x2, waiting for transfers between devices, copy_for_each(): return lax.all_to_all(copies, axis, split_axis=0, concat_axis=0, tiled=True)  96.2 us
    all_to_all x2, starting transfers between devices, copy_for_each(): return lax.all_to_all(copies, axis, split_axis=0, concat_axis=0, tiled=True)  49.1 us
    all_gather x1, waiting for transfers between devices, in_one_piece(): lax.all_gather(both, axis, axis=dim, tiled=True)  12.6 us
  transfers between devices with their start and end apart: 6, of which 6 were waited for; matrix products, arithmetic and copies ran while one was open for 2% of the time, Pallas kernels for 0%

commit v1 on v0

--- a/solution.py
+++ b/solution.py
@@ -4,6 +4,19 @@
 from jax.sharding import PartitionSpec as P
 
 EPS = 1e-06
+
+
+def ring_gather(shard, axis, dim):
+    ways = lax.axis_size(axis)
+    up = [(d, (d + 1) % ways) for d in range(ways)]
+    down = [(d, (d - 1) % ways) for d in range(ways)]
+    earlier, later = ([shard], [shard])
+    for _ in range(ways // 2):
+        earlier.append(lax.ppermute(earlier[-1], axis, up))
+    for _ in range((ways - 1) // 2):
+        later.append(lax.ppermute(later[-1], axis, down))
+    line = jnp.concatenate([*earlier[::-1], *later[1:]], axis=dim)
+    return jnp.roll(line, (lax.axis_index(axis) - ways // 2) * shard.shape[dim], axis=dim)
 
 
 def passed_along(x, axis, by):
@@ -75,7 +88,7 @@
         before = jnp.zeros((conv_reach, channels), jnp.float32)
         conv = convolve(carried, before, conv_taps[layer_index])
         mixed = (gate.astype(jnp.float32) * conv).astype(jnp.bfloat16)
-        mixed_all = lax.all_gather(mixed, "tp", axis=1, tiled=True)
+        mixed_all = ring_gather(mixed, "tp", 1)
         product = jnp.dot(mixed_all, gathered[3][layer_index], preferred_element_type=jnp.float32)
         stream = (stream.astype(jnp.float32) + product).astype(jnp.bfloat16)
     return stream[fringe_depth:]

time: 307 us -> 292 us (0.951)
  the two profiles are of different devices: /device:TPU:66 before, /device:TPU:78 now
where the time goes in v1:
time: 292 us; the launch traced here: 291 us
  waiting for transfers between devices  147 us (50%)
  starting transfers between devices  104 us (36%)
  between operations  13.9 us (5%)
  matrix products  12 us (4%)
  local copies, waits for them, and re-layouts  8.54 us (3%)
  other arithmetic  5.66 us (2%)
    all_to_all x2, waiting for transfers between devices, copy_for_each(): return lax.all_to_all(copies, axis, split_axis=0, concat_axis=0, tiled=True)  89.5 us
    all_to_all x2, starting transfers between devices, copy_for_each(): return lax.all_to_all(copies, axis, split_axis=0, concat_axis=0, tiled=True)  49.8 us
    ppermute x8, starting transfers between devices, ring_gather(): earlier.append(lax.ppermute(earlier[-1], axis, up))  40.6 us
    ppermute x8, waiting for transfers between devices, ring_gather(): earlier.append(lax.ppermute(earlier[-1], axis, up))  26.9 us
    all_gather x1, waiting for transfers between devices, in_one_piece(): lax.all_gather(both, axis, axis=dim, tiled=True)  17.2 us
    ppermute x6, waiting for transfers between devices, ring_gather(): later.append(lax.ppermute(later[-1], axis, down))  12.3 us
    ppermute x6, starting transfers between devices, ring_gather(): later.append(lax.ppermute(later[-1], axis, down))  12.2 us
  transfers between devices with their start and end apart: 18, of which 16 were waited for; matrix products, arithmetic and copies ran while one was open for 2% of the time, Pallas kernels for 0%

profile of v1, /device:TPU:78, one launch (start us, length us, event | category | flops | bytes accessed | tf_op | source)
XLA Modules:
  0.0 291.3 jit_solution(17690352403935190446)
XLA Ops:
  9.0 1.8 collective-permute-start
  14.2 42.7 %all-to-all-start = ((bf16[8,516,256]{2,1,0:T(8,128)(2,1)}), bf16[8,516,256]{2,1,0:T(8,128)(2,1)S(1)}, u32[]{:S(2)}, u32[]{:S(2)}) async-start(bf16[8,516,256]{2,1,0:T(8,128)(2,1)} %broadcast_in_dim.4), calls=%async_computation | async-start | bytes 4259840 | tf_op jit(solution)/shard_map/all_to_all | solution.py:45
  56.9 46.6 %all-to-all-done = bf16[8,516,256]{2,1,0:T(8,128)(2,1)S(1)} async-done(((bf16[8,516,256]{2,1,0:T(8,128)(2,1)}), bf16[8,516,256]{2,1,0:T(8,128)(2,1)S(1)}, u32[]{:S(2)}, u32[]{:S(2)}) %all-to-all-start) | async-done | bytes 2113568 | tf_op jit(solution)/shard_map/all_to_all | solution.py:45
  105.9 17.2 %all-gather.2.cloned.1.call-done = bf16[8,2048,256]{2,1,0:T(8,128)(2,1)} async-done(((bf16[8,64,256]{2,1,0:T(8,128)(2,1)}), bf16[8,2048,256]{2,1,0:T(8,128)(2,1)}) %all-gather.2.cloned.1.call-update) | async-done | bytes 8388624 | tf_op jit(solution)/shard_map/all_gather | solution.py:34
  123.1 2.0 fusion.22
  125.1 2.0 fusion.21
  127.2 2.0 fusion.19
  129.2 2.4 collective-permute-start.1
  131.5 8.1 %collective-permute-done.1 = bf16[516,256]{1,0:T(8,128)(2,1)S(1)} collective-permute-done((bf16[516,256]{1,0:T(8,128)(2,1)S(1)}, bf16[516,256]{1,0:T(8,128)(2,1)S(1)}, u32[]{:S(2)}, u32[]{:S(2)}) %collective-permute-start.1) | collective-permute-done | bytes 264224 | tf_op jit(solution)/shard_map/ppermute | solution.py:15
  139.6 3.6 %collective-permute-start.2 = (bf16[516,256]{1,0:T(8,128)(2,1)S(1)}, bf16[516,256]{1,0:T(8,128)(2,1)S(1)}, u32[]{:S(2)}, u32[]{:S(2)}) collective-permute-start(bf16[516,256]{1,0:T(8,128)(2,1)S(1)} %collective-permute-done.1), channel_id=1, source_target_pairs={{0,1},{1,2},{2,3},{3,4},{4,5},{5,6},{6,7},{7,0},{8,9},{9,10},{10,1... | collective-permute-start | bytes 792584 | tf_op jit(solution)/shard_map/ppermute | solution.py:15
  143.2 2.3 collective-permute-start.5
  145.5 3.7 %collective-permute-done.2 = bf16[516,256]{1,0:T(8,128)(2,1)S(1)} collective-permute-done((bf16[516,256]{1,0:T(8,128)(2,1)S(1)}, bf16[516,256]{1,0:T(8,128)(2,1)S(1)}, u32[]{:S(2)}, u32[]{:S(2)}) %collective-permute-start.2) | collective-permute-done | bytes 264224 | tf_op jit(solution)/shard_map/ppermute | solution.py:15
  149.2 4.8 %collective-permute-start.3 = (bf16[516,256]{1,0:T(8,128)(2,1)S(1)}, bf16[516,256]{1,0:T(8,128)(2,1)S(1)}, u32[]{:S(2)}, u32[]{:S(2)}) collective-permute-start(bf16[516,256]{1,0:T(8,128)(2,1)S(1)} %collective-permute-done.2), channel_id=1, source_target_pairs={{0,1},{1,2},{2,3},{3,4},{4,5},{5,6},{6,7},{7,0},{8,9},{9,10},{10,1... | collective-permute-start | bytes 792584 | tf_op jit(solution)/shard_map/ppermute | solution.py:15
  154.0 2.0 collective-permute-start.6
  156.0 2.3 collective-permute-done.3
  158.3 5.6 %collective-permute-start.4 = (bf16[516,256]{1,0:T(8,128)(2,1)S(1)}, bf16[516,256]{1,0:T(8,128)(2,1)S(1)}, u32[]{:S(2)}, u32[]{:S(2)}) collective-permute-start(bf16[516,256]{1,0:T(8,128)(2,1)S(1)} %collective-permute-done.3), channel_id=1, source_target_pairs={{0,1},{1,2},{2,3},{3,4},{4,5},{5,6},{6,7},{7,0},{8,9},{9,10},{10,1... | collective-permute-start | bytes 792584 | tf_op jit(solution)/shard_map/ppermute | solution.py:15
  164.0 2.1 collective-permute-start.7
  168.1 5.6 %collective-permute-done.7 = bf16[516,256]{1,0:T(8,128)(2,1)S(1)} collective-permute-done((bf16[516,256]{1,0:T(8,128)(2,1)S(1)}, bf16[516,256]{1,0:T(8,128)(2,1)S(1)}, u32[]{:S(2)}, u32[]{:S(2)}) %collective-permute-start.7) | collective-permute-done | bytes 264224 | tf_op jit(solution)/shard_map/ppermute | solution.py:17
  173.7 2.5 fusion.29
  177.8 7.1 %all-to-all-start.1 = ((bf16[8,516,256]{2,1,0:T(8,128)(2,1)}), bf16[8,516,256]{2,1,0:T(8,128)(2,1)S(1)}, u32[]{:S(2)}, u32[]{:S(2)}) async-start(bf16[8,516,256]{2,1,0:T(8,128)(2,1)} %broadcast_in_dim.5), calls=%async_computation.1 | async-start | bytes 4259840 | tf_op jit(solution)/shard_map/all_to_all | solution.py:45
  184.9 42.9 %all-to-all-done.1 = bf16[8,516,256]{2,1,0:T(8,128)(2,1)S(1)} async-done(((bf16[8,516,256]{2,1,0:T(8,128)(2,1)}), bf16[8,516,256]{2,1,0:T(8,128)(2,1)S(1)}, u32[]{:S(2)}, u32[]{:S(2)}) %all-to-all-start.1) | async-done | bytes 2113568 | tf_op jit(solution)/shard_map/all_to_all | solution.py:45
  234.1 7.4 %collective-permute-start.8 = (bf16[516,256]{1,0:T(8,128)(2,1)S(1)}, bf16[516,256]{1,0:T(8,128)(2,1)S(1)}, u32[]{:S(2)}, u32[]{:S(2)}) collective-permute-start(bf16[516,256]{1,0:T(8,128)(2,1)S(1)} %fusion.25), channel_id=1, source_target_pairs={{0,1},{1,2},{2,3},{3,4},{4,5},{5,6},{6,7},{7,0},{8,9},{9,10},{10,1... | collective-permute-start | bytes 792584 | tf_op jit(solution)/shard_map/ppermute | solution.py:15
  241.5 3.9 %collective-permute-done.8 = bf16[516,256]{1,0:T(8,128)(2,1)S(1)} collective-permute-done((bf16[516,256]{1,0:T(8,128)(2,1)S(1)}, bf16[516,256]{1,0:T(8,128)(2,1)S(1)}, u32[]{:S(2)}, u32[]{:S(2)}) %collective-permute-start.8) | collective-permute-done | bytes 264224 | tf_op jit(solution)/shard_map/ppermute | solution.py:15
  245.4 5.6 %collective-permute-start.9 = (bf16[516,256]{1,0:T(8,128)(2,1)S(1)}, bf16[516,256]{1,0:T(8,128)(2,1)S(1)}, u32[]{:S(2)}, u32[]{:S(2)}) collective-permute-start(bf16[516,256]{1,0:T(8,128)(2,1)S(1)} %collective-permute-done.8), channel_id=1, source_target_pairs={{0,1},{1,2},{2,3},{3,4},{4,5},{5,6},{6,7},{7,0},{8,9},{9,10},{10,1... | collective-permute-start | bytes 792584 | tf_op jit(solution)/shard_map/ppermute | solution.py:15
  251.0 2.0 collective-permute-start.12
  253.0 2.4 collective-permute-done.9
  255.4 5.6 %collective-permute-start.10 = (bf16[516,256]{1,0:T(8,128)(2,1)S(1)}, bf16[516,256]{1,0:T(8,128)(2,1)S(1)}, u32[]{:S(2)}, u32[]{:S(2)}) collective-permute-start(bf16[516,256]{1,0:T(8,128)(2,1)S(1)} %collective-permute-done.9), channel_id=1, source_target_pairs={{0,1},{1,2},{2,3},{3,4},{4,5},{5,6},{6,7},{7,0},{8,9},{9,10},{10,1... | collective-permute-start | bytes 792584 | tf_op jit(solution)/shard_map/ppermute | solution.py:15
  261.3 1.9 collective-permute-start.13
  263.3 3.3 %collective-permute-done.10 = bf16[516,256]{1,0:T(8,128)(2,1)S(1)} collective-permute-done((bf16[516,256]{1,0:T(8,128)(2,1)S(1)}, bf16[516,256]{1,0:T(8,128)(2,1)S(1)}, u32[]{:S(2)}, u32[]{:S(2)}) %collective-permute-start.10) | collective-permute-done | bytes 264224 | tf_op jit(solution)/shard_map/ppermute | solution.py:15
  266.6 5.6 %collective-permute-start.11 = (bf16[516,256]{1,0:T(8,128)(2,1)S(1)}, bf16[516,256]{1,0:T(8,128)(2,1)S(1)}, u32[]{:S(2)}, u32[]{:S(2)}) collective-permute-start(bf16[516,256]{1,0:T(8,128)(2,1)S(1)} %collective-permute-done.10), channel_id=1, source_target_pairs={{0,1},{1,2},{2,3},{3,4},{4,5},{5,6},{6,7},{7,0},{8,9},{9,10},{10,1... | collective-permute-start | bytes 792584 | tf_op jit(solution)/shard_map/ppermute | solution.py:15
  272.7 1.9 collective-permute-start.14
  276.4 5.9 %collective-permute-done.14 = bf16[516,256]{1,0:T(8,128)(2,1)S(1)} collective-permute-done((bf16[516,256]{1,0:T(8,128)(2,1)S(1)}, bf16[516,256]{1,0:T(8,128)(2,1)S(1)}, u32[]{:S(2)}, u32[]{:S(2)}) %collective-permute-start.14) | collective-permute-done | bytes 264224 | tf_op jit(solution)/shard_map/ppermute | solution.py:17
  (62 shorter events, 22.5 us)
Async XLA Ops:
  6.5 116.6 %all-gather.2.cloned.1.call-start = ((), (), s32[]{:S(2)}) async-start(), calls=%async_computation.2 | async-start | bytes 8650752 | tf_op jit(solution)/shard_map/all_gather | solution.py:34
  9.0 2.6 collective-permute-start
  14.2 42.7 %copy-start.1 = (bf16[2,2048]{1,0:T(2,128)(2,1)S(1)}, bf16[2,2048]{1,0:T(2,128)(2,1)}, u32[]{:S(2)}) copy-start(bf16[2,2048]{1,0:T(2,128)(2,1)} %param.10) | copy-start | bytes 24580
  14.2 42.7 %copy-start.2 = (bf16[2,3,256]{2,0,1:T(2,128)(2,1)S(1)}, bf16[2,3,256]{2,0,1:T(2,128)(2,1)}, u32[]{:S(2)}) copy-start(bf16[2,3,256]{2,0,1:T(2,128)(2,1)} %param.15) | copy-start | bytes 9220
  14.2 89.4 %all-to-all-start = ((bf16[8,516,256]{2,1,0:T(8,128)(2,1)}), bf16[8,516,256]{2,1,0:T(8,128)(2,1)S(1)}, u32[]{:S(2)}, u32[]{:S(2)}) async-start(bf16[8,516,256]{2,1,0:T(8,128)(2,1)} %broadcast_in_dim.4), calls=%async_computation | async-start | bytes 4259840 | tf_op jit(solution)/shard_map/all_to_all | solution.py:45
  129.2 10.4 %collective-permute-start.1 = (bf16[516,256]{1,0:T(8,128)(2,1)S(1)}, bf16[516,256]{1,0:T(8,128)(2,1)S(1)}, u32[]{:S(2)}, u32[]{:S(2)}) collective-permute-start(bf16[516,256]{1,0:T(8,128)(2,1)S(1)} %fusion.19), channel_id=1, source_target_pairs={{0,1},{1,2},{2,3},{3,4},{4,5},{5,6},{6,7},{7,0},{8,9},{9,10},{10,1... | collective-permute-start | bytes 792584 | tf_op jit(solution)/shard_map/ppermute | solution.py:15
  139.6 9.6 %collective-permute-start.2 = (bf16[516,256]{1,0:T(8,128)(2,1)S(1)}, bf16[516,256]{1,0:T(8,128)(2,1)S(1)}, u32[]{:S(2)}, u32[]{:S(2)}) collective-permute-start(bf16[516,256]{1,0:T(8,128)(2,1)S(1)} %collective-permute-done.1), channel_id=1, source_target_pairs={{0,1},{1,2},{2,3},{3,4},{4,5},{5,6},{6,7},{7,0},{8,9},{9,10},{10,1... | collective-permute-start | bytes 792584 | tf_op jit(solution)/shard_map/ppermute | solution.py:15
  143.2 10.8 %collective-permute-start.5 = (bf16[516,256]{1,0:T(8,128)(2,1)S(1)}, bf16[516,256]{1,0:T(8,128)(2,1)S(1)}, u32[]{:S(2)}, u32[]{:S(2)}) collective-permute-start(bf16[516,256]{1,0:T(8,128)(2,1)S(1)} %fusion.19), channel_id=1, source_target_pairs={{0,7},{1,0},{2,1},{3,2},{4,3},{5,4},{6,5},{7,6},{8,15},{9,8},{10,9... | collective-permute-start | bytes 792584 | tf_op jit(solution)/shard_map/ppermute | solution.py:17
  149.2 9.1 %collective-permute-start.3 = (bf16[516,256]{1,0:T(8,128)(2,1)S(1)}, bf16[516,256]{1,0:T(8,128)(2,1)S(1)}, u32[]{:S(2)}, u32[]{:S(2)}) collective-permute-start(bf16[516,256]{1,0:T(8,128)(2,1)S(1)} %collective-permute-done.2), channel_id=1, source_target_pairs={{0,1},{1,2},{2,3},{3,4},{4,5},{5,6},{6,7},{7,0},{8,9},{9,10},{10,1... | collective-permute-start | bytes 792584 | tf_op jit(solution)/shard_map/ppermute | solution.py:15
  154.0 10.0 %collective-permute-start.6 = (bf16[516,256]{1,0:T(8,128)(2,1)S(1)}, bf16[516,256]{1,0:T(8,128)(2,1)S(1)}, u32[]{:S(2)}, u32[]{:S(2)}) collective-permute-start(bf16[516,256]{1,0:T(8,128)(2,1)S(1)} %collective-permute-done.5), channel_id=1, source_target_pairs={{0,7},{1,0},{2,1},{3,2},{4,3},{5,4},{6,5},{7,6},{8,15},{9,8},{10,9... | collective-permute-start | bytes 792584 | tf_op jit(solution)/shard_map/ppermute | solution.py:17
  158.3 9.5 %collective-permute-start.4 = (bf16[516,256]{1,0:T(8,128)(2,1)S(1)}, bf16[516,256]{1,0:T(8,128)(2,1)S(1)}, u32[]{:S(2)}, u32[]{:S(2)}) collective-permute-start(bf16[516,256]{1,0:T(8,128)(2,1)S(1)} %collective-permute-done.3), channel_id=1, source_target_pairs={{0,1},{1,2},{2,3},{3,4},{4,5},{5,6},{6,7},{7,0},{8,9},{9,10},{10,1... | collective-permute-start | bytes 792584 | tf_op jit(solution)/shard_map/ppermute | solution.py:15
  163.9 9.7 %copy-start = (bf16[512,256]{1,0:T(8,128)(2,1)S(1)}, bf16[512,256]{1,0:T(8,128)(2,1)}, u32[]{:S(2)}) copy-start(bf16[512,256]{1,0:T(8,128)(2,1)} %param.9) | copy-start | bytes 786436
  164.0 9.7 %collective-permute-start.7 = (bf16[516,256]{1,0:T(8,128)(2,1)S(1)}, bf16[516,256]{1,0:T(8,128)(2,1)S(1)}, u32[]{:S(2)}, u32[]{:S(2)}) collective-permute-start(bf16[516,256]{1,0:T(8,128)(2,1)S(1)} %collective-permute-done.6), channel_id=1, source_target_pairs={{0,7},{1,0},{2,1},{3,2},{4,3},{5,4},{6,5},{7,6},{8,15},{9,8},{10,9... | collective-permute-start | bytes 792584 | tf_op jit(solution)/shard_map/ppermute | solution.py:17
  177.8 50.0 %all-to-all-start.1 = ((bf16[8,516,256]{2,1,0:T(8,128)(2,1)}), bf16[8,516,256]{2,1,0:T(8,128)(2,1)S(1)}, u32[]{:S(2)}, u32[]{:S(2)}) async-start(bf16[8,516,256]{2,1,0:T(8,128)(2,1)} %broadcast_in_dim.5), calls=%async_computation.1 | async-start | bytes 4259840 | tf_op jit(solution)/shard_map/all_to_all | solution.py:45
  228.3 2.2 slice-start
  228.8 3.0 %slice-start.1 = ((s8[8388608]{0:T(1024)(128)(4,1)}), s8[4194304]{0:T(1024)(128)(4,1)S(1)}, s32[]{:S(2)}) async-start(s8[8388608]{0:T(1024)(128)(4,1)} %bitcast.60), calls=%async_computation.4 | async-start | bytes 8388608
  234.1 11.3 %collective-permute-start.8 = (bf16[516,256]{1,0:T(8,128)(2,1)S(1)}, bf16[516,256]{1,0:T(8,128)(2,1)S(1)}, u32[]{:S(2)}, u32[]{:S(2)}) collective-permute-start(bf16[516,256]{1,0:T(8,128)(2,1)S(1)} %fusion.25), channel_id=1, source_target_pairs={{0,1},{1,2},{2,3},{3,4},{4,5},{5,6},{6,7},{7,0},{8,9},{9,10},{10,1... | collective-permute-start | bytes 792584 | tf_op jit(solution)/shard_map/ppermute | solution.py:15
  245.4 10.0 %collective-permute-start.9 = (bf16[516,256]{1,0:T(8,128)(2,1)S(1)}, bf16[516,256]{1,0:T(8,128)(2,1)S(1)}, u32[]{:S(2)}, u32[]{:S(2)}) collective-permute-start(bf16[516,256]{1,0:T(8,128)(2,1)S(1)} %collective-permute-done.8), channel_id=1, source_target_pairs={{0,1},{1,2},{2,3},{3,4},{4,5},{5,6},{6,7},{7,0},{8,9},{9,10},{10,1... | collective-permute-start | bytes 792584 | tf_op jit(solution)/shard_map/ppermute | solution.py:15
  251.0 10.3 %collective-permute-start.12 = (bf16[516,256]{1,0:T(8,128)(2,1)S(1)}, bf16[516,256]{1,0:T(8,128)(2,1)S(1)}, u32[]{:S(2)}, u32[]{:S(2)}) collective-permute-start(bf16[516,256]{1,0:T(8,128)(2,1)S(1)} %fusion.25), channel_id=1, source_target_pairs={{0,7},{1,0},{2,1},{3,2},{4,3},{5,4},{6,5},{7,6},{8,15},{9,8},{10,9... | collective-permute-start | bytes 792584 | tf_op jit(solution)/shard_map/ppermute | solution.py:17
  255.4 11.2 %collective-permute-start.10 = (bf16[516,256]{1,0:T(8,128)(2,1)S(1)}, bf16[516,256]{1,0:T(8,128)(2,1)S(1)}, u32[]{:S(2)}, u32[]{:S(2)}) collective-permute-start(bf16[516,256]{1,0:T(8,128)(2,1)S(1)} %collective-permute-done.9), channel_id=1, source_target_pairs={{0,1},{1,2},{2,3},{3,4},{4,5},{5,6},{6,7},{7,0},{8,9},{9,10},{10,1... | collective-permute-start | bytes 792584 | tf_op jit(solution)/shard_map/ppermute | solution.py:15
  261.3 11.4 %collective-permute-start.13 = (bf16[516,256]{1,0:T(8,128)(2,1)S(1)}, bf16[516,256]{1,0:T(8,128)(2,1)S(1)}, u32[]{:S(2)}, u32[]{:S(2)}) collective-permute-start(bf16[516,256]{1,0:T(8,128)(2,1)S(1)} %collective-permute-done.12), channel_id=1, source_target_pairs={{0,7},{1,0},{2,1},{3,2},{4,3},{5,4},{6,5},{7,6},{8,15},{9,8},{10,9... | collective-permute-start | bytes 792584 | tf_op jit(solution)/shard_map/ppermute | solution.py:17
  266.6 9.5 %collective-permute-start.11 = (bf16[516,256]{1,0:T(8,128)(2,1)S(1)}, bf16[516,256]{1,0:T(8,128)(2,1)S(1)}, u32[]{:S(2)}, u32[]{:S(2)}) collective-permute-start(bf16[516,256]{1,0:T(8,128)(2,1)S(1)} %collective-permute-done.10), channel_id=1, source_target_pairs={{0,1},{1,2},{2,3},{3,4},{4,5},{5,6},{6,7},{7,0},{8,9},{9,10},{10,1... | collective-permute-start | bytes 792584 | tf_op jit(solution)/shard_map/ppermute | solution.py:15
  272.7 9.5 %collective-permute-start.14 = (bf16[516,256]{1,0:T(8,128)(2,1)S(1)}, bf16[516,256]{1,0:T(8,128)(2,1)S(1)}, u32[]{:S(2)}, u32[]{:S(2)}) collective-permute-start(bf16[516,256]{1,0:T(8,128)(2,1)S(1)} %collective-permute-done.13), channel_id=1, source_target_pairs={{0,7},{1,0},{2,1},{3,2},{4,3},{5,4},{6,5},{7,6},{8,15},{9,8},{10,9... | collective-permute-start | bytes 792584 | tf_op jit(solution)/shard_map/ppermute | solution.py:17
Sparse Core Ops, SparseCore 0:
  9.5 113.5 all-gather.1
